TPU v7x, 256 devices: a whole 4x4x8 slice. The times are simulated.
256 devices in a mesh: ep: 16 (over y, x), tp: 16 (over z, core).
Axes of the slice: x: 4, y: 4, z: 8, core: 2. Of those that a mesh axis runs over, the one named last changes fastest.
Arguments:
- mix_tokens: bfloat16 [16384, 1, 1024], P(('ep', 'tp')), may hold values from -6 to 6
- mix_gain: float32 [1024], replicated, may hold values from 0.1 to 1.9
- w_query: bfloat16 [1024, 1024], replicated, may hold values from -0.1875 to 0.1875
- w_key: bfloat16 [1024, 256], replicated, may hold values from -0.1875 to 0.1875
- w_value: bfloat16 [1024, 256], replicated, may hold values from -0.1875 to 0.1875
- query_gain: float32 [64], replicated, may hold values from 1.2 to 14
- key_gain: float32 [64], replicated, may hold values from 1.2 to 14
- w_out: bfloat16 [1024, 1024], replicated, may hold values from -0.1875 to 0.1875
- expert_tokens: bfloat16 [32768, 1024], P(('ep', 'tp')), may hold values from -6 to 6
- expert_gain: float32 [1024], replicated, may hold values from 0.1 to 1.9
- route_ids: int32 [32768, 2], P(('ep', 'tp')), may hold values from 0 to 31, all different within a row; in each aligned block of 128 rows (0 to 127, 128 to 255, ...) at most 9 rows name the same one
- route_weights: float32 [32768, 2], P(('ep', 'tp')), may hold values from 0.1 to 1
- w_gate: bfloat16 [32, 1024, 4096], P('ep', None, 'tp'), may hold values from -0.1875 to 0.1875
- w_up: bfloat16 [32, 1024, 4096], P('ep', None, 'tp'), may hold values from -0.1875 to 0.1875
- w_down: bfloat16 [32, 4096, 1024], P('ep', 'tp'), may hold values from -0.09375 to 0.09375
Outputs:
- mix_out: bfloat16 [16384, 1, 1024], P(('ep', 'tp'))
- experts_out: bfloat16 [32768, 1024], P(('ep', 'tp'))
Inputs may be any that keep to these rules, and one draw needn't show every extreme that they name: `route_ids`: each row names 2 different experts. Among the rows of one device no expert is named more than 9 times, and in every draw some expert is named exactly 9 times by the rows of some device.
All inputs are finite; a program needn't handle non-finite values.
Results may differ from a plain program's by a relative error of at most 0.018.
The roundings to bfloat16 on the way count: a program that leaves them out, or rounds other values in their place, can miss the bound.
Values may be sent and summed in bfloat16 or wider, within the bound.
A program may use at most 128 MiB of HBM per device.

v0:
```python
import math
import jax
import jax.numpy as jnp
from jax import lax
from jax.sharding import PartitionSpec as P

HEAD = 64
GRID_W = 64
epsilon = 1e-06


def normalize(values, gain_vec):
    widened = values.astype(jnp.float32)
    return (
        widened
        * lax.rsqrt(jnp.mean(widened * widened, axis=-1, keepdims=True) + epsilon)
        * gain_vec
    )


def angle_tables(positions, head_size):
    quarter = head_size // 4
    frequency = 10000.0 ** (-jnp.arange(quarter, dtype=jnp.float32) / quarter)
    grid_pos = jnp.stack([positions // GRID_W, positions % GRID_W], axis=-1).astype(jnp.float32)
    angles = grid_pos[:, :, None] * frequency[None, None, :]
    return (jnp.cos(angles), jnp.sin(angles))


def turn(values, cosine_table, sine_table):
    shaped = values.shape
    quarter = shaped[-1] // 4
    leading = (shaped[0],) + (1,) * (len(shaped) - 2) + (2, quarter)
    cosine_table = cosine_table.reshape(leading)
    sine_table = sine_table.reshape(leading)
    halves = values.reshape(shaped[:-1] + (2, 2, quarter))
    first_part = halves[..., 0, :]
    second_part = halves[..., 1, :]
    turned = jnp.stack(
        [
            first_part * cosine_table - second_part * sine_table,
            first_part * sine_table + second_part * cosine_table,
        ],
        axis=-2,
    )
    return turned.reshape(shaped)


def attend(queries, fold_state, key_piece):
    key_rows = key_piece.shape[0]
    block_rows = math.gcd(key_rows, 1024)
    blocks = key_piece.reshape((key_rows // block_rows, block_rows) + key_piece.shape[1:])
    score_scale = HEAD ** (-0.5)

    def step_block(carried, block_keys):
        running_max, totals, accumulated = carried
        keys_part = block_keys[..., :HEAD]
        values_part = block_keys[..., HEAD:]
        scores = (
            jnp.einsum("qshd,ksd->qshk", queries, keys_part, preferred_element_type=jnp.float32)
            * score_scale
        )
        new_max = jnp.maximum(running_max, jnp.max(scores, axis=-1))
        shrink = jnp.exp(running_max - new_max)
        raised = jnp.exp(scores - new_max[..., None])
        totals = totals * shrink + jnp.sum(raised, axis=-1)
        accumulated = accumulated * shrink[..., None] + jnp.einsum(
            "qshk,ksd->qshd",
            raised.astype(jnp.bfloat16),
            values_part,
            preferred_element_type=jnp.float32,
        )
        return ((new_max, totals, accumulated), None)

    return lax.scan(step_block, fold_state, blocks)[0]


def mixer_half(mix_tokens, mix_gain, w_query, w_key, w_value, query_gain, key_gain, w_out):
    tp_count = lax.axis_size("tp")
    seq_rows, sequences, model_width = mix_tokens.shape
    head_count = w_query.shape[1] // HEAD
    key_heads = w_key.shape[1] // HEAD
    local_heads = head_count // tp_count
    normed = normalize(mix_tokens, mix_gain).astype(jnp.bfloat16)
    queries = jnp.dot(normed, w_query, preferred_element_type=jnp.float32).astype(jnp.bfloat16)
    keys_raw = jnp.dot(normed, w_key, preferred_element_type=jnp.float32).astype(jnp.bfloat16)
    values = jnp.dot(normed, w_value, preferred_element_type=jnp.float32).astype(jnp.bfloat16)
    queries = queries.reshape(seq_rows, sequences, tp_count, local_heads * HEAD)
    key_value = jnp.concatenate(
        [
            keys_raw.reshape(seq_rows, sequences, key_heads, HEAD),
            values.reshape(seq_rows, sequences, key_heads, HEAD),
        ],
        axis=-1,
    )
    key_value = jnp.repeat(key_value, tp_count // key_heads, axis=2)
    packed = jnp.concatenate([queries, key_value], axis=-1)
    arrived = lax.all_to_all(packed, "tp", split_axis=2, concat_axis=0, tiled=True)
    span_rows = arrived.shape[0]
    positions = lax.axis_index("ep") * span_rows + jnp.arange(span_rows, dtype=jnp.int32)
    cosine_table, sine_table = angle_tables(positions, HEAD)
    query_width = local_heads * HEAD
    own_queries = normalize(
        arrived[:, :, 0, :query_width].reshape(span_rows, sequences, local_heads, HEAD), query_gain
    )
    own_queries = turn(own_queries, cosine_table, sine_table).astype(jnp.bfloat16)
    own_keys = normalize(arrived[:, :, 0, query_width : query_width + HEAD], key_gain)
    own_keys = turn(own_keys, cosine_table, sine_table).astype(jnp.bfloat16)
    key_pairs = jnp.concatenate([own_keys, arrived[:, :, 0, query_width + HEAD :]], axis=-1)
    start_state = (
        jnp.full((span_rows, sequences, local_heads), -1e30, jnp.float32),
        jnp.zeros((span_rows, sequences, local_heads), jnp.float32),
        jnp.zeros((span_rows, sequences, local_heads, HEAD), jnp.float32),
    )
    running_max, totals, accumulated = attend(
        own_queries, start_state, lax.all_gather(key_pairs, "ep", axis=0, tiled=True)
    )
    mixed = (
        (accumulated / totals[..., None])
        .astype(jnp.bfloat16)
        .reshape(span_rows, sequences, query_width)
    )
    returned = lax.all_to_all(mixed, "tp", split_axis=0, concat_axis=2, tiled=True)
    return jnp.dot(returned, w_out, preferred_element_type=jnp.float32).astype(jnp.bfloat16)


def joint_hidden(w_gate, w_up, piece_rows):
    gate_act = jnp.einsum("rjd,jdf->rjf", piece_rows, w_gate, preferred_element_type=jnp.float32)
    up_act = jnp.einsum("rjd,jdf->rjf", piece_rows, w_up, preferred_element_type=jnp.float32)
    return (jax.nn.silu(gate_act) * up_act).astype(jnp.bfloat16)


def joint_down(hidden_all, w_down):
    group_sum = jnp.einsum(
        "rjf,jfd->rjd", hidden_all, w_down, preferred_element_type=jnp.float32
    ).astype(jnp.bfloat16)
    return lax.optimization_barrier(group_sum).astype(jnp.float32)


def expert_half(expert_tokens, expert_gain, route_ids, route_weights, w_gate, w_up, w_down):
    ep_count = lax.axis_size("ep")
    tok_count, model_width = expert_tokens.shape
    top_count = route_ids.shape[1]
    local_experts = w_gate.shape[0]
    expert_count = local_experts * ep_count
    capacity = tok_count * top_count * 9 // (8 * expert_count)
    slot_count = ep_count * capacity * local_experts
    normed = normalize(expert_tokens, expert_gain).astype(jnp.bfloat16)
    flat_ids = route_ids.reshape(-1)
    matches = (flat_ids[:, None] == jnp.arange(expert_count, dtype=jnp.int32)[None, :]).astype(
        jnp.int32
    )
    rank_ids = jnp.sum((jnp.cumsum(matches, axis=0) - 1) * matches, axis=1)
    slot_ids = (
        flat_ids // local_experts * capacity + rank_ids
    ) * local_experts + flat_ids % local_experts
    chosen = slot_ids.reshape(tok_count, top_count)
    dispatch = jnp.sum(
        (chosen[:, :, None] == jnp.arange(slot_count, dtype=jnp.int32)[None, None, :]).astype(
            jnp.bfloat16
        ),
        axis=1,
    )
    outgoing = lax.dot_general(
        dispatch, normed, (((0,), (0,)), ((), ())), preferred_element_type=jnp.float32
    )
    outgoing = outgoing.astype(jnp.bfloat16).reshape(ep_count, capacity, local_experts, model_width)
    incoming = lax.all_to_all(outgoing, "ep", split_axis=0, concat_axis=0, tiled=True)
    own_rows = ep_count * capacity
    incoming = incoming.reshape(own_rows, local_experts, model_width)
    hidden_all = joint_hidden(w_gate, w_up, lax.all_gather(incoming, "tp", axis=0, tiled=True))
    summed = lax.psum_scatter(
        joint_down(hidden_all, w_down).astype(jnp.bfloat16), "tp", scatter_dimension=0, tiled=True
    )
    expert_results = summed.reshape(ep_count, capacity, local_experts, model_width)
    returned = lax.all_to_all(
        expert_results, "ep", split_axis=0, concat_axis=0, tiled=True
    ).reshape(slot_count, model_width)
    picked = jnp.take(returned, slot_ids, axis=0).reshape(tok_count, top_count, model_width)
    combined = jnp.sum(route_weights[:, :, None] * picked.astype(jnp.float32), axis=1)
    return combined.astype(jnp.bfloat16)


def body(
    mix_tokens,
    mix_gain,
    w_query,
    w_key,
    w_value,
    query_gain,
    key_gain,
    w_out,
    expert_tokens,
    expert_gain,
    route_ids,
    route_weights,
    w_gate,
    w_up,
    w_down,
):
    mix_out = mixer_half(mix_tokens, mix_gain, w_query, w_key, w_value, query_gain, key_gain, w_out)
    experts_out = expert_half(
        expert_tokens, expert_gain, route_ids, route_weights, w_gate, w_up, w_down
    )
    return (mix_out, experts_out)


def solution(mesh):
    placed = (
        P(("ep", "tp"), None, None),
        P(),
        P(),
        P(),
        P(),
        P(),
        P(),
        P(),
        P(("ep", "tp"), None),
        P(),
        P(("ep", "tp"), None),
        P(("ep", "tp"), None),
        P("ep", None, "tp"),
        P("ep", None, "tp"),
        P("ep", "tp", None),
    )
    return jax.shard_map(
        body,
        mesh=mesh,
        in_specs=placed,
        out_specs=(P(("ep", "tp"), None, None), P(("ep", "tp"), None)),
        check_vma=False,
    )
```

profile of v0, /device:TPU:1, one launch (start us, length us, event | category | flops | bytes accessed | tf_op | source)
XLA Modules:
  0.0 339.7 jit_solution(8806245419591874709)
XLA Ops:
  11.5 1.3 convolution_convert_fusion
  13.0 18.7 %all_to_all.43 = bf16[16,9,2,1024]{3,2,1,0:T(2,128)(2,1)S(1)} all-to-all(bf16[16,9,2,1024]{3,2,1,0:T(2,128)(2,1)S(1)} %reshape.571), channel_id=1, replica_groups=mesh['ep'=16,'tp'=16] {'ep'}, dimensions={0} | all-to-all | bytes 1179648 | tf_op jit(solution)/shard_map/all_to_all | solution.py:167
  37.7 10.4 %all-to-all-start = ((bf16[64,1,16,192]{3,0,1,2:T(8,128)(2,1)}), bf16[64,1,16,192]{3,0,1,2:T(8,128)(2,1)S(1)}, u32[]{:S(2)}, u32[]{:S(2)}) async-start(bf16[64,1,16,192]{3,0,1,2:T(8,128)(2,1)} %pad_maximum_fusion), calls=%async_computation | async-start | bytes 1048576 | tf_op jit(solution)/shard_map/all_to_all | solution.py:97
  48.3 22.1 %all-to-all-done = bf16[64,1,16,192]{3,0,1,2:T(8,128)(2,1)S(1)} async-done(((bf16[64,1,16,192]{3,0,1,2:T(8,128)(2,1)}), bf16[64,1,16,192]{3,0,1,2:T(8,128)(2,1)S(1)}, u32[]{:S(2)}, u32[]{:S(2)}) %all-to-all-start) | async-done | bytes 393248 | tf_op jit(solution)/shard_map/all_to_all | solution.py:97
  77.2 28.6 %all-gather.5.cloned.1.call-done = bf16[2304,2,1024]{2,0,1:T(8,128)(2,1)} async-done(((bf16[144,2,1024]{2,0,1:T(8,128)(2,1)}), bf16[2304,2,1024]{2,0,1:T(8,128)(2,1)}) %all-gather.5.cloned.1.call-update) | async-done | bytes 9437200 | tf_op jit(solution)/shard_map/all_gather | solution.py:170
  105.8 8.7 %convolution_bitcast_fusion.1 = f32[2304,2,256]{2,0,1:T(8,128)} fusion(bf16[2304,2,1024]{2,0,1:T(8,128)(2,1)} %all-gather.5.cloned.1.call-done, bf16[2,1024,256]{2,1,0:T(8,128)(2,1)} %param.29), kind=kOutput, calls=%fused_computation.26 | convolution fusion | flops 2415919104 | bytes 15204352 | tf_op jit(solution)/shard_map/rjd,jdf->rjf/dot_general | solution.py:127
  114.5 11.7 %convert_bitcast_fusion = bf16[2304,2,1024]{2,0,1:T(8,128)(2,1)} fusion(bf16[2,256,1024]{2,1,0:T(8,128)(2,1)} %param.31, bf16[2304,2,1024]{2,0,1:T(8,128)(2,1)} %all-gather.5.cloned.1.call-done, bf16[2,1024,256]{2,1,0:T(8,128)(2,1)} %param.30, f32[2304,2,256]{2,0,1:T(8,128)} %convolution_bitcast_fusion.1), kind=kOutput, calls=%fused_computation.23 | convolution fusion | flops 4843634688 | bytes 25690112 | tf_op jit(solution)/shard_map/rjf,jfd->rjd/dot_general | solution.py:133
  126.2 36.4 %all-gather.3.cloned.1.call-done = bf16[16384,1,128]{2,0,1:T(8,128)(2,1)} async-done(((bf16[1024,1,128]{2,0,1:T(8,128)(2,1)}), bf16[16384,1,128]{2,0,1:T(8,128)(2,1)}) %all-gather.3.cloned.1.call-update) | async-done | bytes 4194320 | tf_op jit(solution)/shard_map/all_gather | solution.py:115
  162.7 131.4 %while.15 = (s32[]{:T(128)}, f32[1024,1,1]{0,2,1:T(1,128)S(1)}, f32[1024,1,1]{0,2,1:T(1,128)S(1)}, f32[1024,1,1,64]{0,3,2,1:T(8,128)S(1)}, bf16[16,1024,1,128]{3...) while((s32[]{:T(128)}, f32[1024,1,1]{0,2,1:T(1,128)S(1)}, ...), condition=%wide.region_6.7_spmd.clone, body=%wide.region_3.6_spmd.clone.sunk | while | flops 277025792 | bytes 31129728 | solution.py:74
  163.6 2.7 multiply_reduce_fusion.4
  166.4 3.1 fusion.81
  171.7 2.7 multiply_reduce_fusion.4
  174.5 3.2 fusion.81
  180.3 2.7 multiply_reduce_fusion.4
  183.0 3.2 fusion.81
  188.6 2.7 multiply_reduce_fusion.4
  191.3 3.2 fusion.81
  196.9 2.7 multiply_reduce_fusion.4
  199.6 3.2 fusion.81
  205.2 2.7 multiply_reduce_fusion.4
  207.9 3.2 fusion.81
  213.5 2.7 multiply_reduce_fusion.4
  216.2 3.2 fusion.81
  221.8 2.7 multiply_reduce_fusion.4
  224.5 3.2 fusion.81
  230.1 2.7 multiply_reduce_fusion.4
  232.8 3.2 fusion.81
  238.3 2.7 multiply_reduce_fusion.4
  241.1 3.1 fusion.81
  246.4 2.7 multiply_reduce_fusion.4
  249.2 3.1 fusion.81
  254.5 2.7 multiply_reduce_fusion.4
  257.3 3.1 fusion.81
  262.6 2.7 multiply_reduce_fusion.4
  265.4 3.1 fusion.81
  270.7 2.7 multiply_reduce_fusion.4
  273.5 3.1 fusion.81
  278.8 2.7 multiply_reduce_fusion.4
  281.6 3.1 fusion.81
  286.9 2.7 multiply_reduce_fusion.4
  289.7 3.1 fusion.81
  296.4 7.9 %all-to-all-start.1 = ((bf16[16,2,2048]{2,1,0:T(2,128)(2,1)}), bf16[16,2,2048]{2,1,0:T(2,128)(2,1)S(1)}, u32[]{:S(2)}, u32[]{:S(2)}) async-start(bf16[16,2,2048]{2,1,0:T(2,128)(2,1)} %reshape.590), calls=%async_computation.1 | async-start | bytes 262144 | tf_op jit(solution)/shard_map/all_to_all | solution.py:122
  304.7 2.5 copy.149
  307.1 6.0 %all-to-all-done.1 = bf16[16,2,2048]{2,1,0:T(2,128)(2,1)S(1)} async-done(((bf16[16,2,2048]{2,1,0:T(2,128)(2,1)}), bf16[16,2,2048]{2,1,0:T(2,128)(2,1)S(1)}, u32[]{:S(2)}, u32[]{:S(2)}) %all-to-all-start.1) | async-done | bytes 131104 | tf_op jit(solution)/shard_map/all_to_all | solution.py:122
  313.1 4.2 %all-to-all-start.3 = ((bf16[16,9,2,1024]{3,2,1,0:T(2,128)(2,1)}), bf16[16,9,2,1024]{3,2,1,0:T(2,128)(2,1)S(1)}, u32[]{:S(2)}, u32[]{:S(2)}) async-start(bf16[16,9,2,1024]{3,2,1,0:T(2,128)(2,1)} %bitcast.24), calls=%async_computation.4 | async-start | bytes 1179648 | tf_op jit(solution)/shard_map/all_to_all | solution.py:175
  318.8 2.7 fusion.20
  321.5 7.7 %all-to-all-done.3 = bf16[16,9,2,1024]{3,2,1,0:T(2,128)(2,1)S(1)} async-done(((bf16[16,9,2,1024]{3,2,1,0:T(2,128)(2,1)}), bf16[16,9,2,1024]{3,2,1,0:T(2,128)(2,1)S(1)}, u32[]{:S(2)}, u32[]{:S(2)}) %all-to-all-start.3) | async-done | bytes 589856 | tf_op jit(solution)/shard_map/all_to_all | solution.py:175
  330.8 2.4 multiply_reduce_fusion.1
  (201 shorter events, 60.3 us)
Async XLA Ops:
  7.2 28.7 %copy-start = (bf16[1024,1024]{1,0:T(8,128)(2,1)S(1)}, bf16[1024,1024]{1,0:T(8,128)(2,1)}, u32[]{:S(2)}) copy-start(bf16[1024,1024]{1,0:T(8,128)(2,1)} %param.19) | copy-start | bytes 6291460
  7.2 25.5 %copy-start.2 = (bf16[64,1,1024]{2,0,1:T(8,128)(2,1)S(1)}, bf16[64,1,1024]{2,0,1:T(8,128)(2,1)}, u32[]{:S(2)}) copy-start(bf16[64,1,1024]{2,0,1:T(8,128)(2,1)} %param.17) | copy-start | bytes 393220
  7.2 25.7 %copy-start.3 = (f32[1024]{0:T(1024)S(1)}, f32[1024]{0:T(1024)}, u32[]{:S(2)}) copy-start(f32[1024]{0:T(1024)} %param.18) | copy-start | bytes 12292
  7.2 98.6 %all-gather.5.cloned.1.call-start = ((), (), s32[]{:S(2)}) async-start(), calls=%async_computation.6 | async-start | bytes 10027008 | tf_op jit(solution)/shard_map/all_gather | solution.py:170
  32.7 15.4 %copy-start.6 = (f32[64]{0:T(128)S(1)}, f32[64]{0:T(128)}, u32[]{:S(2)}) copy-start(f32[64]{0:T(128)} %param.23) | copy-start | bytes 772
  36.7 39.9 %copy-start.5 = (f32[64]{0:T(128)S(1)}, f32[64]{0:T(128)}, u32[]{:S(2)}) copy-start(f32[64]{0:T(128)} %param.22) | copy-start | bytes 772
  37.7 32.7 %all-to-all-start = ((bf16[64,1,16,192]{3,0,1,2:T(8,128)(2,1)}), bf16[64,1,16,192]{3,0,1,2:T(8,128)(2,1)S(1)}, u32[]{:S(2)}, u32[]{:S(2)}) async-start(bf16[64,1,16,192]{3,0,1,2:T(8,128)(2,1)} %pad_maximum_fusion), calls=%async_computation | async-start | bytes 1048576 | tf_op jit(solution)/shard_map/all_to_all | solution.py:97
  48.1 114.6 %all-gather.3.cloned.1.call-start = ((), (), s32[]{:S(2)}) async-start(), calls=%async_computation.5 | async-start | bytes 4456448 | tf_op jit(solution)/shard_map/all_gather | solution.py:115
  75.1 229.5 %reduce-scatter.2.cloned.1.call-start = ((), (), s32[]{:S(2)}) async-start(), calls=%async_computation.7 | async-start | bytes 10027008 | tf_op jit(solution)/shard_map/reduce_scatter | solution.py:171
  162.7 141.9 %copy-start.4 = (f32[128,2]{0,1:T(2,128)S(1)}, f32[128,2]{0,1:T(2,128)}, u32[]{:S(2)}) copy-start(f32[128,2]{0,1:T(2,128)} %param.28) | copy-start | bytes 3076
  166.4 3.4 %copy-start.1 = (f32[1024,1024]{1,0:T(8,128)S(1)}, f32[1024,1024]{1,0:T(8,128)}, u32[]{:S(2)}) copy-start(f32[1024,1024]{1,0:T(8,128)} %get-tuple-element.163) | copy-start | bytes 12582916 | tf_op jit(solution)/shard_map/while
  174.5 3.9 %copy-start.1 = (f32[1024,1024]{1,0:T(8,128)S(1)}, f32[1024,1024]{1,0:T(8,128)}, u32[]{:S(2)}) copy-start(f32[1024,1024]{1,0:T(8,128)} %get-tuple-element.163) | copy-start | bytes 12582916 | tf_op jit(solution)/shard_map/while
  183.0 3.6 %copy-start.1 = (f32[1024,1024]{1,0:T(8,128)S(1)}, f32[1024,1024]{1,0:T(8,128)}, u32[]{:S(2)}) copy-start(f32[1024,1024]{1,0:T(8,128)} %get-tuple-element.163) | copy-start | bytes 12582916 | tf_op jit(solution)/shard_map/while
  191.3 3.6 %copy-start.1 = (f32[1024,1024]{1,0:T(8,128)S(1)}, f32[1024,1024]{1,0:T(8,128)}, u32[]{:S(2)}) copy-start(f32[1024,1024]{1,0:T(8,128)} %get-tuple-element.163) | copy-start | bytes 12582916 | tf_op jit(solution)/shard_map/while
  199.6 3.6 %copy-start.1 = (f32[1024,1024]{1,0:T(8,128)S(1)}, f32[1024,1024]{1,0:T(8,128)}, u32[]{:S(2)}) copy-start(f32[1024,1024]{1,0:T(8,128)} %get-tuple-element.163) | copy-start | bytes 12582916 | tf_op jit(solution)/shard_map/while
  207.9 3.6 %copy-start.1 = (f32[1024,1024]{1,0:T(8,128)S(1)}, f32[1024,1024]{1,0:T(8,128)}, u32[]{:S(2)}) copy-start(f32[1024,1024]{1,0:T(8,128)} %get-tuple-element.163) | copy-start | bytes 12582916 | tf_op jit(solution)/shard_map/while
  216.2 3.6 %copy-start.1 = (f32[1024,1024]{1,0:T(8,128)S(1)}, f32[1024,1024]{1,0:T(8,128)}, u32[]{:S(2)}) copy-start(f32[1024,1024]{1,0:T(8,128)} %get-tuple-element.163) | copy-start | bytes 12582916 | tf_op jit(solution)/shard_map/while
  224.5 3.6 %copy-start.1 = (f32[1024,1024]{1,0:T(8,128)S(1)}, f32[1024,1024]{1,0:T(8,128)}, u32[]{:S(2)}) copy-start(f32[1024,1024]{1,0:T(8,128)} %get-tuple-element.163) | copy-start | bytes 12582916 | tf_op jit(solution)/shard_map/while
  232.8 3.6 %copy-start.1 = (f32[1024,1024]{1,0:T(8,128)S(1)}, f32[1024,1024]{1,0:T(8,128)}, u32[]{:S(2)}) copy-start(f32[1024,1024]{1,0:T(8,128)} %get-tuple-element.163) | copy-start | bytes 12582916 | tf_op jit(solution)/shard_map/while
  241.0 3.4 %copy-start.1 = (f32[1024,1024]{1,0:T(8,128)S(1)}, f32[1024,1024]{1,0:T(8,128)}, u32[]{:S(2)}) copy-start(f32[1024,1024]{1,0:T(8,128)} %get-tuple-element.163) | copy-start | bytes 12582916 | tf_op jit(solution)/shard_map/while
  249.1 3.4 %copy-start.1 = (f32[1024,1024]{1,0:T(8,128)S(1)}, f32[1024,1024]{1,0:T(8,128)}, u32[]{:S(2)}) copy-start(f32[1024,1024]{1,0:T(8,128)} %get-tuple-element.163) | copy-start | bytes 12582916 | tf_op jit(solution)/shard_map/while
  257.2 3.4 %copy-start.1 = (f32[1024,1024]{1,0:T(8,128)S(1)}, f32[1024,1024]{1,0:T(8,128)}, u32[]{:S(2)}) copy-start(f32[1024,1024]{1,0:T(8,128)} %get-tuple-element.163) | copy-start | bytes 12582916 | tf_op jit(solution)/shard_map/while
  265.4 3.4 %copy-start.1 = (f32[1024,1024]{1,0:T(8,128)S(1)}, f32[1024,1024]{1,0:T(8,128)}, u32[]{:S(2)}) copy-start(f32[1024,1024]{1,0:T(8,128)} %get-tuple-element.163) | copy-start | bytes 12582916 | tf_op jit(solution)/shard_map/while
  273.5 3.4 %copy-start.1 = (f32[1024,1024]{1,0:T(8,128)S(1)}, f32[1024,1024]{1,0:T(8,128)}, u32[]{:S(2)}) copy-start(f32[1024,1024]{1,0:T(8,128)} %get-tuple-element.163) | copy-start | bytes 12582916 | tf_op jit(solution)/shard_map/while
  281.6 3.4 %copy-start.1 = (f32[1024,1024]{1,0:T(8,128)S(1)}, f32[1024,1024]{1,0:T(8,128)}, u32[]{:S(2)}) copy-start(f32[1024,1024]{1,0:T(8,128)} %get-tuple-element.163) | copy-start | bytes 12582916 | tf_op jit(solution)/shard_map/while
  289.7 3.4 %copy-start.1 = (f32[1024,1024]{1,0:T(8,128)S(1)}, f32[1024,1024]{1,0:T(8,128)}, u32[]{:S(2)}) copy-start(f32[1024,1024]{1,0:T(8,128)} %get-tuple-element.163) | copy-start | bytes 12582916 | tf_op jit(solution)/shard_map/while
  296.4 16.8 %all-to-all-start.1 = ((bf16[16,2,2048]{2,1,0:T(2,128)(2,1)}), bf16[16,2,2048]{2,1,0:T(2,128)(2,1)S(1)}, u32[]{:S(2)}, u32[]{:S(2)}) async-start(bf16[16,2,2048]{2,1,0:T(2,128)(2,1)} %reshape.590), calls=%async_computation.1 | async-start | bytes 262144 | tf_op jit(solution)/shard_map/all_to_all | solution.py:122
  313.1 16.1 %all-to-all-start.3 = ((bf16[16,9,2,1024]{3,2,1,0:T(2,128)(2,1)}), bf16[16,9,2,1024]{3,2,1,0:T(2,128)(2,1)S(1)}, u32[]{:S(2)}, u32[]{:S(2)}) async-start(bf16[16,9,2,1024]{3,2,1,0:T(2,128)(2,1)} %bitcast.24), calls=%async_computation.4 | async-start | bytes 1179648 | tf_op jit(solution)/shard_map/all_to_all | solution.py:175
Sparse Core Ops, SparseCore 0:
  32.8 72.8 all-gather.4
  108.2 54.3 all-gather.2
  165.2 69.8 reduce-scatter.1
where the time goes:
time: 341 us; the launch traced here: 340 us
  waiting for transfers between devices  101 us (30%)
  matrix products  85.9 us (25%)
  other arithmetic  61.8 us (18%)
  local copies, waits for them, and re-layouts  35 us (10%)
  starting transfers between devices  22.7 us (7%)
  blocking collectives  18.7 us (5%)
  between operations  14.2 us (4%)
    reduce_sum x16, other arithmetic, step_block(): totals = totals * shrink + jnp.sum(raised, axis=-1)  50 us
    dot_general x16, matrix products, step_block(): jnp.einsum('qshd,ksd->qshk', queries, keys_part, preferred_element_type=j...  43.4 us
    all_gather x1, waiting for transfers between devices, mixer_half(): lax.all_gather(key_pairs, 'ep', axis=0, tiled=True)  36.4 us
    all_gather x1, waiting for transfers between devices, expert_half(): lax.all_gather(incoming, 'tp', axis=0, tiled=True)  28.6 us
    all_to_all x1, waiting for transfers between devices, mixer_half(): lax.all_to_all(packed, 'tp', split_axis=2, concat_axis=0, tiled=True)  22.1 us
    all_to_all x1, blocking collectives, expert_half(): lax.all_to_all(outgoing, 'ep', split_axis=0, concat_axis=0, tiled=True)  18.7 us
    squeeze x16, local copies, waits for them, and re-layouts, attend(): return lax.scan(step_block, fold_state, blocks)[0]  15.6 us
    dot_general x16, matrix products, step_block(): jnp.einsum('qshk,ksd->qshd', raised.astype(jnp.bfloat16), values_part, pr...  14.9 us
  transfers between devices with their start and end apart: 6, of which 5 were waited for; matrix products, arithmetic and copies ran while one was open for 49% of the time, Pallas kernels for 0%

commit v1 on v0

--- a/solution.py
+++ b/solution.py
@@ -112,7 +112,11 @@
         jnp.zeros((span_rows, sequences, local_heads, HEAD), jnp.float32),
     )
     running_max, totals, accumulated = attend(
-        own_queries, start_state, lax.all_gather(key_pairs, "ep", axis=0, tiled=True)
+        own_queries,
+        start_state,
+        jnp.concatenate(
+            lax.all_to_all(jnp.stack([key_pairs] * lax.axis_size("ep")), "ep", 0, 0), axis=0
+        ),
     )
     mixed = (
         (accumulated / totals[..., None])

time: 341 us -> 321 us (0.941)
  waiting for transfers between devices: 101 us -> 79 us
    all_gather x1 -> x0, waiting for transfers between devices: 36.4 us -> none  [mixer_half(): lax.all_gather(key_pairs, 'ep', axis=0, tiled=True)]
    all_to_all x0 -> x1, waiting for transfers between devices: none -> 20.4 us  [mixer_half(): lax.all_to_all(jnp.stack([key_pairs] * lax.axis_size('ep')), 'ep', 0, 0)]
    all_gather x1, waiting for transfers between devices: 28.6 us -> 22.7 us  [expert_half(): lax.all_gather(incoming, 'tp', axis=0, tiled=True)]
    all_to_all x0 -> x1, starting transfers between devices: none -> 4.69 us  [mixer_half(): lax.all_to_all(jnp.stack([key_pairs] * lax.axis_size('ep')), 'ep', 0, 0)]
    all_to_all x1, starting transfers between devices: 7.87 us -> 4.34 us  [mixer_half(): lax.all_to_all(mixed, 'tp', split_axis=0, concat_axis=2, tiled=True)]
  transfers between devices with their start and end apart: 6 -> 6, of which waited for: 5 -> 5; matrix products, arithmetic and copies ran while one was open for 49% -> 52% of each run, Pallas kernels for 0% -> 0%
where the time goes in v1:
time: 321 us; the launch traced here: 320 us
  matrix products  85.9 us (27%)
  waiting for transfers between devices  79 us (25%)
  other arithmetic  60.8 us (19%)
  local copies, waits for them, and re-layouts  36.5 us (11%)
  starting transfers between devices  23.5 us (7%)
  blocking collectives  18.7 us (6%)
  between operations  14.5 us (5%)
    reduce_sum x16, other arithmetic, step_block(): totals = totals * shrink + jnp.sum(raised, axis=-1)  49.7 us
    dot_general x16, matrix products, step_block(): jnp.einsum('qshd,ksd->qshk', queries, keys_part, preferred_element_type=j...  43.4 us
    all_gather x1, waiting for transfers between devices, expert_half(): lax.all_gather(incoming, 'tp', axis=0, tiled=True)  22.7 us
    all_to_all x1, waiting for transfers between devices, mixer_half(): lax.all_to_all(packed, 'tp', split_axis=2, concat_axis=0, tiled=True)  22.2 us
    all_to_all x1, waiting for transfers between devices, mixer_half(): lax.all_to_all(jnp.stack([key_pairs] * lax.axis_size('ep')), 'ep', 0, 0)  20.4 us
    all_to_all x1, blocking collectives, expert_half(): lax.all_to_all(outgoing, 'ep', split_axis=0, concat_axis=0, tiled=True)  18.7 us
    squeeze x16, local copies, waits for them, and re-layouts, attend(): return lax.scan(step_block, fold_state, blocks)[0]  15.6 us
    dot_general x16, matrix products, step_block(): jnp.einsum('qshk,ksd->qshd', raised.astype(jnp.bfloat16), values_part, pr...  14.9 us
  transfers between devices with their start and end apart: 6, of which 5 were waited for; matrix products, arithmetic and copies ran while one was open for 52% of the time, Pallas kernels for 0%

profile of v1, /device:TPU:1, one launch (start us, length us, event | category | flops | bytes accessed | tf_op | source)
XLA Modules:
  0.0 319.6 jit_solution(18382692328158582175)
XLA Ops:
  13.0 18.7 %all_to_all.48 = bf16[16,9,2,1024]{3,2,1,0:T(2,128)(2,1)S(1)} all-to-all(bf16[16,9,2,1024]{3,2,1,0:T(2,128)(2,1)S(1)} %reshape.570), channel_id=1, replica_groups=mesh['ep'=16,'tp'=16] {'ep'}, dimensions={0} | all-to-all | bytes 1179648 | tf_op jit(solution)/shard_map/all_to_all | solution.py:171
  37.7 10.4 %all-to-all-start = ((bf16[64,1,16,192]{3,0,1,2:T(8,128)(2,1)}), bf16[64,1,16,192]{3,0,1,2:T(8,128)(2,1)S(1)}, u32[]{:S(2)}, u32[]{:S(2)}) async-start(bf16[64,1,16,192]{3,0,1,2:T(8,128)(2,1)} %pad_maximum_fusion), calls=%async_computation | async-start | bytes 1048576 | tf_op jit(solution)/shard_map/all_to_all | solution.py:97
  48.2 22.2 %all-to-all-done = bf16[64,1,16,192]{3,0,1,2:T(8,128)(2,1)S(1)} async-done(((bf16[64,1,16,192]{3,0,1,2:T(8,128)(2,1)}), bf16[64,1,16,192]{3,0,1,2:T(8,128)(2,1)S(1)}, u32[]{:S(2)}, u32[]{:S(2)}) %all-to-all-start) | async-done | bytes 393248 | tf_op jit(solution)/shard_map/all_to_all | solution.py:97
  74.4 2.9 stack.12
  77.3 4.7 %all-to-all-start.1 = ((bf16[16,1024,1,128]{3,1,2,0:T(8,128)(2,1)}), bf16[16,1024,1,128]{3,1,2,0:T(8,128)(2,1)}, u32[]{:S(2)}, u32[]{:S(2)}) async-start(bf16[16,1024,1,128]{3,1,2,0:T(8,128)(2,1)} %stack.12), calls=%async_computation.1 | async-start | bytes 8388608 | tf_op jit(solution)/shard_map/all_to_all | solution.py:118
  83.1 22.7 %all-gather.2.cloned.1.call-done = bf16[2304,2,1024]{2,0,1:T(8,128)(2,1)} async-done(((bf16[144,2,1024]{2,0,1:T(8,128)(2,1)}), bf16[2304,2,1024]{2,0,1:T(8,128)(2,1)}) %all-gather.2.cloned.1.call-update) | async-done | bytes 9437200 | tf_op jit(solution)/shard_map/all_gather | solution.py:174
  105.8 8.7 %convolution_bitcast_fusion.1 = f32[2304,2,256]{2,0,1:T(8,128)} fusion(bf16[2304,2,1024]{2,0,1:T(8,128)(2,1)} %all-gather.2.cloned.1.call-done, bf16[2,1024,256]{2,1,0:T(8,128)(2,1)} %param.29), kind=kOutput, calls=%fused_computation.26 | convolution fusion | flops 2415919104 | bytes 15204352 | tf_op jit(solution)/shard_map/rjd,jdf->rjf/dot_general | solution.py:131
  114.5 11.7 %convert_bitcast_fusion = bf16[2304,2,1024]{2,0,1:T(8,128)(2,1)} fusion(bf16[2,256,1024]{2,1,0:T(8,128)(2,1)} %param.31, bf16[2304,2,1024]{2,0,1:T(8,128)(2,1)} %all-gather.2.cloned.1.call-done, bf16[2,1024,256]{2,1,0:T(8,128)(2,1)} %param.30, f32[2304,2,256]{2,0,1:T(8,128)} %convolution_bitcast_fusion.1), kind=kOutput, calls=%fused_computation.23 | convolution fusion | flops 4843634688 | bytes 25690112 | tf_op jit(solution)/shard_map/rjf,jfd->rjd/dot_general | solution.py:137
  126.2 20.4 %all-to-all-done.1 = bf16[16,1024,1,128]{3,1,2,0:T(8,128)(2,1)} async-done(((bf16[16,1024,1,128]{3,1,2,0:T(8,128)(2,1)}), bf16[16,1024,1,128]{3,1,2,0:T(8,128)(2,1)}, u32[]{:S(2)}, u32[]{:S(2)}) %all-to-all-start.1) | async-done | bytes 4194336 | tf_op jit(solution)/shard_map/all_to_all | solution.py:118
  146.7 130.8 %while.15 = (s32[]{:T(128)}, f32[1024,1,1]{0,2,1:T(1,128)S(1)}, f32[1024,1,1]{0,2,1:T(1,128)S(1)}, f32[1024,1,1,64]{0,3,2,1:T(8,128)S(1)}, bf16[16,1024,1,128]{3...) while((s32[]{:T(128)}, f32[1024,1,1]{0,2,1:T(1,128)S(1)}, ...), condition=%wide.region_6.7_spmd.clone, body=%wide.region_3.6_spmd.clone.sunk | while | flops 277025792 | bytes 31129728 | solution.py:74
  147.7 2.7 multiply_reduce_fusion.4
  150.4 3.2 fusion.81
  156.0 2.7 multiply_reduce_fusion.4
  158.7 3.2 fusion.81
  164.3 2.7 multiply_reduce_fusion.4
  167.0 3.2 fusion.81
  172.6 2.7 multiply_reduce_fusion.4
  175.3 3.2 fusion.81
  180.8 2.7 multiply_reduce_fusion.4
  183.6 3.2 fusion.81
  189.1 2.7 multiply_reduce_fusion.4
  191.9 3.2 fusion.81
  197.4 2.7 multiply_reduce_fusion.4
  200.2 3.1 fusion.81
  205.5 2.7 multiply_reduce_fusion.4
  208.3 3.1 fusion.81
  213.6 2.7 multiply_reduce_fusion.4
  216.4 3.1 fusion.81
  221.7 2.7 multiply_reduce_fusion.4
  224.5 3.1 fusion.81
  229.8 2.7 multiply_reduce_fusion.4
  232.6 3.1 fusion.81
  237.9 2.7 multiply_reduce_fusion.4
  240.7 3.1 fusion.81
  246.0 2.7 multiply_reduce_fusion.4
  248.8 3.1 fusion.81
  254.1 2.7 multiply_reduce_fusion.4
  256.9 3.1 fusion.81
  262.2 2.7 multiply_reduce_fusion.4
  265.0 3.1 fusion.81
  270.3 2.7 multiply_reduce_fusion.4
  273.1 3.1 fusion.81
  279.8 4.3 %all-to-all-start.2 = ((bf16[16,2,2048]{2,1,0:T(2,128)(2,1)}), bf16[16,2,2048]{2,1,0:T(2,128)(2,1)S(1)}, u32[]{:S(2)}, u32[]{:S(2)}) async-start(bf16[16,2,2048]{2,1,0:T(2,128)(2,1)} %reshape.589), calls=%async_computation.2 | async-start | bytes 262144 | tf_op jit(solution)/shard_map/all_to_all | solution.py:126
  284.5 2.5 copy.143
  287.0 6.0 %all-to-all-done.2 = bf16[16,2,2048]{2,1,0:T(2,128)(2,1)S(1)} async-done(((bf16[16,2,2048]{2,1,0:T(2,128)(2,1)}), bf16[16,2,2048]{2,1,0:T(2,128)(2,1)S(1)}, u32[]{:S(2)}, u32[]{:S(2)}) %all-to-all-start.2) | async-done | bytes 131104 | tf_op jit(solution)/shard_map/all_to_all | solution.py:126
  293.0 3.9 %all-to-all-start.4 = ((bf16[16,9,2,1024]{3,2,1,0:T(2,128)(2,1)}), bf16[16,9,2,1024]{3,2,1,0:T(2,128)(2,1)S(1)}, u32[]{:S(2)}, u32[]{:S(2)}) async-start(bf16[16,9,2,1024]{3,2,1,0:T(2,128)(2,1)} %bitcast.23), calls=%async_computation.5 | async-start | bytes 1179648 | tf_op jit(solution)/shard_map/all_to_all | solution.py:179
  298.4 2.7 fusion.20
  301.1 7.7 %all-to-all-done.4 = bf16[16,9,2,1024]{3,2,1,0:T(2,128)(2,1)S(1)} async-done(((bf16[16,9,2,1024]{3,2,1,0:T(2,128)(2,1)}), bf16[16,9,2,1024]{3,2,1,0:T(2,128)(2,1)S(1)}, u32[]{:S(2)}, u32[]{:S(2)}) %all-to-all-start.4) | async-done | bytes 589856 | tf_op jit(solution)/shard_map/all_to_all | solution.py:179
  (203 shorter events, 62.0 us)
Async XLA Ops:
  7.2 28.7 %copy-start = (bf16[1024,1024]{1,0:T(8,128)(2,1)S(1)}, bf16[1024,1024]{1,0:T(8,128)(2,1)}, u32[]{:S(2)}) copy-start(bf16[1024,1024]{1,0:T(8,128)(2,1)} %param.19) | copy-start | bytes 6291460
  7.2 25.5 %copy-start.2 = (bf16[64,1,1024]{2,0,1:T(8,128)(2,1)S(1)}, bf16[64,1,1024]{2,0,1:T(8,128)(2,1)}, u32[]{:S(2)}) copy-start(bf16[64,1,1024]{2,0,1:T(8,128)(2,1)} %param.17) | copy-start | bytes 393220
  7.2 25.7 %copy-start.4 = (f32[1024]{0:T(1024)S(1)}, f32[1024]{0:T(1024)}, u32[]{:S(2)}) copy-start(f32[1024]{0:T(1024)} %param.18) | copy-start | bytes 12292
  7.2 98.6 %all-gather.2.cloned.1.call-start = ((), (), s32[]{:S(2)}) async-start(), calls=%async_computation.6 | async-start | bytes 10027008 | tf_op jit(solution)/shard_map/all_gather | solution.py:174
  32.7 15.4 %copy-start.7 = (f32[64]{0:T(128)S(1)}, f32[64]{0:T(128)}, u32[]{:S(2)}) copy-start(f32[64]{0:T(128)} %param.23) | copy-start | bytes 772
  37.7 32.7 %all-to-all-start = ((bf16[64,1,16,192]{3,0,1,2:T(8,128)(2,1)}), bf16[64,1,16,192]{3,0,1,2:T(8,128)(2,1)S(1)}, u32[]{:S(2)}, u32[]{:S(2)}) async-start(bf16[64,1,16,192]{3,0,1,2:T(8,128)(2,1)} %pad_maximum_fusion), calls=%async_computation | async-start | bytes 1048576 | tf_op jit(solution)/shard_map/all_to_all | solution.py:97
  77.3 5.0 %copy-start.3 = (bf16[1024,1,1,64]{3,0,2,1:T(8,128)(2,1)S(1)}, bf16[1024,1,1,64]{3,0,2,1:T(8,128)(2,1)}, u32[]{:S(2)}) copy-start(bf16[1024,1,1,64]{3,0,2,1:T(8,128)(2,1)} %get-tuple-element.76) | copy-start | bytes 393220
  77.3 5.2 %copy-start.6 = (f32[64]{0:T(128)S(1)}, f32[64]{0:T(128)}, u32[]{:S(2)}) copy-start(f32[64]{0:T(128)} %param.22) | copy-start | bytes 772
  77.3 69.4 %all-to-all-start.1 = ((bf16[16,1024,1,128]{3,1,2,0:T(8,128)(2,1)}), bf16[16,1024,1,128]{3,1,2,0:T(8,128)(2,1)}, u32[]{:S(2)}, u32[]{:S(2)}) async-start(bf16[16,1024,1,128]{3,1,2,0:T(8,128)(2,1)} %stack.12), calls=%async_computation.1 | async-start | bytes 8388608 | tf_op jit(solution)/shard_map/all_to_all | solution.py:118
  82.0 202.6 %reduce-scatter.2.cloned.1.call-start = ((), (), s32[]{:S(2)}) async-start(), calls=%async_computation.7 | async-start | bytes 10027008 | tf_op jit(solution)/shard_map/reduce_scatter | solution.py:175
  146.7 137.7 %copy-start.5 = (f32[128,2]{0,1:T(2,128)S(1)}, f32[128,2]{0,1:T(2,128)}, u32[]{:S(2)}) copy-start(f32[128,2]{0,1:T(2,128)} %param.28) | copy-start | bytes 3076
  150.4 3.6 %copy-start.1 = (f32[1024,1024]{1,0:T(8,128)S(1)}, f32[1024,1024]{1,0:T(8,128)}, u32[]{:S(2)}) copy-start(f32[1024,1024]{1,0:T(8,128)} %get-tuple-element.127) | copy-start | bytes 12582916 | tf_op jit(solution)/shard_map/while
  158.7 3.6 %copy-start.1 = (f32[1024,1024]{1,0:T(8,128)S(1)}, f32[1024,1024]{1,0:T(8,128)}, u32[]{:S(2)}) copy-start(f32[1024,1024]{1,0:T(8,128)} %get-tuple-element.127) | copy-start | bytes 12582916 | tf_op jit(solution)/shard_map/while
  167.0 3.6 %copy-start.1 = (f32[1024,1024]{1,0:T(8,128)S(1)}, f32[1024,1024]{1,0:T(8,128)}, u32[]{:S(2)}) copy-start(f32[1024,1024]{1,0:T(8,128)} %get-tuple-element.127) | copy-start | bytes 12582916 | tf_op jit(solution)/shard_map/while
  175.3 3.6 %copy-start.1 = (f32[1024,1024]{1,0:T(8,128)S(1)}, f32[1024,1024]{1,0:T(8,128)}, u32[]{:S(2)}) copy-start(f32[1024,1024]{1,0:T(8,128)} %get-tuple-element.127) | copy-start | bytes 12582916 | tf_op jit(solution)/shard_map/while
  183.6 3.6 %copy-start.1 = (f32[1024,1024]{1,0:T(8,128)S(1)}, f32[1024,1024]{1,0:T(8,128)}, u32[]{:S(2)}) copy-start(f32[1024,1024]{1,0:T(8,128)} %get-tuple-element.127) | copy-start | bytes 12582916 | tf_op jit(solution)/shard_map/while
  191.9 3.6 %copy-start.1 = (f32[1024,1024]{1,0:T(8,128)S(1)}, f32[1024,1024]{1,0:T(8,128)}, u32[]{:S(2)}) copy-start(f32[1024,1024]{1,0:T(8,128)} %get-tuple-element.127) | copy-start | bytes 12582916 | tf_op jit(solution)/shard_map/while
  200.1 3.4 %copy-start.1 = (f32[1024,1024]{1,0:T(8,128)S(1)}, f32[1024,1024]{1,0:T(8,128)}, u32[]{:S(2)}) copy-start(f32[1024,1024]{1,0:T(8,128)} %get-tuple-element.127) | copy-start | bytes 12582916 | tf_op jit(solution)/shard_map/while
  208.2 3.4 %copy-start.1 = (f32[1024,1024]{1,0:T(8,128)S(1)}, f32[1024,1024]{1,0:T(8,128)}, u32[]{:S(2)}) copy-start(f32[1024,1024]{1,0:T(8,128)} %get-tuple-element.127) | copy-start | bytes 12582916 | tf_op jit(solution)/shard_map/while
  216.3 3.4 %copy-start.1 = (f32[1024,1024]{1,0:T(8,128)S(1)}, f32[1024,1024]{1,0:T(8,128)}, u32[]{:S(2)}) copy-start(f32[1024,1024]{1,0:T(8,128)} %get-tuple-element.127) | copy-start | bytes 12582916 | tf_op jit(solution)/shard_map/while
  224.5 3.4 %copy-start.1 = (f32[1024,1024]{1,0:T(8,128)S(1)}, f32[1024,1024]{1,0:T(8,128)}, u32[]{:S(2)}) copy-start(f32[1024,1024]{1,0:T(8,128)} %get-tuple-element.127) | copy-start | bytes 12582916 | tf_op jit(solution)/shard_map/while
  232.6 3.4 %copy-start.1 = (f32[1024,1024]{1,0:T(8,128)S(1)}, f32[1024,1024]{1,0:T(8,128)}, u32[]{:S(2)}) copy-start(f32[1024,1024]{1,0:T(8,128)} %get-tuple-element.127) | copy-start | bytes 12582916 | tf_op jit(solution)/shard_map/while
  240.7 3.4 %copy-start.1 = (f32[1024,1024]{1,0:T(8,128)S(1)}, f32[1024,1024]{1,0:T(8,128)}, u32[]{:S(2)}) copy-start(f32[1024,1024]{1,0:T(8,128)} %get-tuple-element.127) | copy-start | bytes 12582916 | tf_op jit(solution)/shard_map/while
  248.8 3.4 %copy-start.1 = (f32[1024,1024]{1,0:T(8,128)S(1)}, f32[1024,1024]{1,0:T(8,128)}, u32[]{:S(2)}) copy-start(f32[1024,1024]{1,0:T(8,128)} %get-tuple-element.127) | copy-start | bytes 12582916 | tf_op jit(solution)/shard_map/while
  256.9 3.4 %copy-start.1 = (f32[1024,1024]{1,0:T(8,128)S(1)}, f32[1024,1024]{1,0:T(8,128)}, u32[]{:S(2)}) copy-start(f32[1024,1024]{1,0:T(8,128)} %get-tuple-element.127) | copy-start | bytes 12582916 | tf_op jit(solution)/shard_map/while
  265.0 3.4 %copy-start.1 = (f32[1024,1024]{1,0:T(8,128)S(1)}, f32[1024,1024]{1,0:T(8,128)}, u32[]{:S(2)}) copy-start(f32[1024,1024]{1,0:T(8,128)} %get-tuple-element.127) | copy-start | bytes 12582916 | tf_op jit(solution)/shard_map/while
  273.1 3.4 %copy-start.1 = (f32[1024,1024]{1,0:T(8,128)S(1)}, f32[1024,1024]{1,0:T(8,128)}, u32[]{:S(2)}) copy-start(f32[1024,1024]{1,0:T(8,128)} %get-tuple-element.127) | copy-start | bytes 12582916 | tf_op jit(solution)/shard_map/while
  279.8 13.2 %all-to-all-start.2 = ((bf16[16,2,2048]{2,1,0:T(2,128)(2,1)}), bf16[16,2,2048]{2,1,0:T(2,128)(2,1)S(1)}, u32[]{:S(2)}, u32[]{:S(2)}) async-start(bf16[16,2,2048]{2,1,0:T(2,128)(2,1)} %reshape.589), calls=%async_computation.2 | async-start | bytes 262144 | tf_op jit(solution)/shard_map/all_to_all | solution.py:126
  293.0 15.7 %all-to-all-start.4 = ((bf16[16,9,2,1024]{3,2,1,0:T(2,128)(2,1)}), bf16[16,9,2,1024]{3,2,1,0:T(2,128)(2,1)S(1)}, u32[]{:S(2)}, u32[]{:S(2)}) async-start(bf16[16,9,2,1024]{3,2,1,0:T(2,128)(2,1)} %bitcast.23), calls=%async_computation.5 | async-start | bytes 1179648 | tf_op jit(solution)/shard_map/all_to_all | solution.py:179
Sparse Core Ops, SparseCore 0:
  32.8 72.8 all-gather.1
  126.4 68.2 reduce-scatter.1
